TPU v7x, 256 devices: a whole 4x4x8 slice. The times are simulated.
256 devices in a mesh: sp: 32 (over z, x), tp: 8 (over y, core).
Axes of the slice: x: 4, y: 4, z: 8, core: 2. Of those that a mesh axis runs over, the one named last changes fastest.
Arguments:
- residual: bfloat16 [24576, 2048], P('sp'), may hold values from -6 to 6
- queries: bfloat16 [24576, 1024], P('sp', 'tp'), may hold values from -12 to 12
- keys: bfloat16 [24576, 512], P('sp', 'tp'), may hold values from -6 to 6
- values: bfloat16 [24576, 512], P('sp', 'tp'), may hold values from -36 to 36
- segments: int32 [24576], P('sp'), may hold values from 0 to 15, never falling along the last dimension, each value on 1 to 3072 neighbouring positions
- sink: float32 [16], P('tp'), may hold values from 3 to 7
- out_weight: bfloat16 [1024, 2048], replicated, may hold values from -0.1875 to 0.1875
- norm_gain_one: float32 [2048], replicated, may hold values from 0.1 to 1.9
- group: int32 [24576], P('sp'), may hold values from 0 to 3, as said below
- member: int32 [24576, 2], P('sp'), may hold values from 0 to 7, as said below
- route_weight: float32 [24576, 2], P('sp'), may hold values from 0.25 to 1
- gate_weight: bfloat16 [32, 2048, 1024], P('sp', None, 'tp'), may hold values from -0.125 to 0.125
- up_weight: bfloat16 [32, 2048, 1024], P('sp', None, 'tp'), may hold values from -0.125 to 0.125
- down_weight: bfloat16 [32, 1024, 2048], P('sp', None, 'tp'), may hold values from -0.1875 to 0.1875
- norm_gain_two: float32 [2048], P('tp'), may hold values from 0.1 to 1.9
Outputs:
- output: bfloat16 [24576, 2048], P('sp', 'tp')
Inputs may be any that keep to these rules, and one draw needn't show every extreme that they name: In every aligned block of 96 rows no expert (group * 8 + member) is named by more than 12 rows, and one expert, the same in all blocks of a draw, is named by exactly 12 rows of every block. `member`: the 2 members of a row differ.
All inputs are finite; a program needn't handle non-finite values.
Results may differ from a plain program's by a relative error of at most 0.0059.
Values may be sent and summed in bfloat16 or wider, within the bound.
No kernel may reach another device: no remote copies, remote signals or barrier semaphores. Data moves between devices by JAX's collectives and lax.ppermute only.
A program may use at most 128 MiB of HBM per device.

v0:
```python
import math
import jax
import jax.numpy as jnp
from jax import lax
from jax.sharding import PartitionSpec as P

HEAD_DIM = 64
HALF = 128
PER_GROUP = 8
ALPHA = 2.0**0.25
EPS = 1e-05


def with_halo(block, sides, width):
    for axis, dim in sides:
        count = lax.axis_size(axis)
        forward = [(i, i + 1) for i in range(count - 1)]
        backward = [(target, source) for source, target in forward]
        low = lax.ppermute(
            lax.slice_in_dim(block, block.shape[dim] - width, None, axis=dim), axis, forward
        )
        high = lax.ppermute(lax.slice_in_dim(block, 0, width, axis=dim), axis, backward)
        block = jnp.concatenate([low, block, high], axis=dim)
    return block


def copy_for_each(x, axis):
    copies = jnp.broadcast_to(x, (lax.axis_size(axis), *x.shape))
    return lax.all_to_all(copies, axis, split_axis=0, concat_axis=0, tiled=True)


def joined_along(pieces, dim):
    pieces = jnp.moveaxis(pieces, 0, dim)
    lengths = pieces.shape
    return pieces.reshape(*lengths[:dim], lengths[dim] * lengths[dim + 1], *lengths[dim + 2 :])


def gather_directly(x, axis, dim):
    pieces = copy_for_each(x, axis)
    return joined_along(pieces, dim)


def taken_together(x, axis):
    everything = copy_for_each(x, axis)
    return jnp.sum(everything, axis=0)


def packed_total(arrays, axis):
    ends = [0]
    for a in arrays:
        ends.append(ends[-1] + a.size)
    subtotal = taken_together(jnp.concatenate([a.ravel() for a in arrays]), axis)
    return tuple((subtotal[b:e].reshape(a.shape) for a, b, e in zip(arrays, ends, ends[1:])))


def layer_norm(summed, norm_gain):
    mean_value = jnp.mean(summed, -1, keepdims=True)
    variance = jnp.mean(jnp.square(summed - mean_value), -1, keepdims=True)
    return ((summed - mean_value) * lax.rsqrt(variance + EPS) * norm_gain).astype(jnp.bfloat16)


def shards(
    residual,
    queries,
    keys,
    values,
    segments,
    sink,
    out_weight,
    norm_gain_one,
    group,
    member,
    route_weight,
    gate_weight,
    up_weight,
    down_weight,
    norm_gain_two,
):
    row_count = queries.shape[0]
    sp_size = lax.axis_size("sp")
    tp_size = lax.axis_size("tp")
    kv_local = keys.shape[1] // HEAD_DIM
    heads_local = queries.shape[1] // HEAD_DIM
    group_size = heads_local // kv_local
    seq_total = row_count * sp_size
    seq_start = lax.axis_index("sp") * row_count
    joined = jnp.concatenate([keys, values], axis=1)
    padded, seg_padded = (
        with_halo(joined, (("sp", 0),), HALF),
        with_halo(segments, (("sp", 0),), HALF),
    )
    query_block = math.gcd(row_count, 512)
    key_span = query_block + 2 * HALF
    offsets = jnp.arange(key_span)[None, :] - HALF - jnp.arange(query_block)[:, None]
    in_band = jnp.abs(offsets) <= HALF
    sink_heads = sink.reshape(kv_local, group_size, 1, 1)
    query_heads = queries.reshape(row_count, kv_local, group_size, HEAD_DIM)
    key_cols = kv_local * HEAD_DIM
    pieces = []
    for number in range(row_count // query_block):
        row_low = number * query_block
        query_rows = query_heads[row_low : row_low + query_block]
        kv_rows = padded[row_low : row_low + key_span]
        key_part = kv_rows[:, :key_cols].reshape(key_span, kv_local, HEAD_DIM)
        value_part = kv_rows[:, key_cols:].reshape(key_span, kv_local, HEAD_DIM)
        key_place = seq_start + row_low - HALF + jnp.arange(key_span)
        inside = (key_place >= 0) & (key_place < seq_total)
        same_doc = (
            segments[row_low : row_low + query_block, None]
            == seg_padded[None, row_low : row_low + key_span]
        )
        allowed = in_band & same_doc & inside[None, :]
        scores = jnp.einsum(
            "qkgd,ckd->kgqc", query_rows, key_part, preferred_element_type=jnp.float32
        ) * HEAD_DIM ** (-0.5)
        masked = jnp.where(allowed, scores, -1e30)
        peak = jnp.maximum(jnp.max(masked, -1, keepdims=True), sink_heads)
        raised = jnp.where(allowed, jnp.exp(masked - peak), 0.0)
        denominator = jnp.sum(raised, -1, keepdims=True) + jnp.exp(sink_heads - peak)
        weights = (raised / denominator).astype(jnp.bfloat16)
        attended_part = jnp.einsum(
            "kgqc,ckd->qkgd", weights, value_part, preferred_element_type=jnp.float32
        )
        pieces.append(
            attended_part.reshape(query_block, heads_local * HEAD_DIM).astype(jnp.bfloat16)
        )
    attended = jnp.concatenate(pieces, 0)
    width = out_weight.shape[1]
    weight_rows = out_weight
    mixed = jnp.dot(
        gather_directly(attended, "tp", 1), weight_rows, preferred_element_type=jnp.float32
    )
    pre_one = ALPHA * residual.astype(jnp.float32) + mixed
    normed = layer_norm(pre_one, norm_gain_one)
    experts_local = gate_weight.shape[0]
    expert_count = experts_local * sp_size
    picks_count = member.shape[1]
    block_rows = row_count // tp_size
    capacity = max(2, block_rows // 8)
    expert_ids = (group[:, None] * PER_GROUP + member).reshape(tp_size, block_rows * picks_count)
    onehot_table = (expert_ids[:, :, None] == jnp.arange(expert_count)[None, None, :]).astype(
        jnp.int32
    )
    ranks = jnp.sum((jnp.cumsum(onehot_table, 1) - 1) * onehot_table, 2)
    owner = expert_ids // experts_local
    local_ids = expert_ids % experts_local
    block_ids = jnp.arange(tp_size)[:, None]
    slot_all = ((local_ids * sp_size + owner) * tp_size + block_ids) * capacity + ranks
    copy_rows = (
        jnp.arange(row_count * picks_count).reshape(tp_size, block_rows * picks_count)
        // picks_count
    )
    extended = jnp.concatenate([normed, jnp.zeros((1, width), jnp.bfloat16)], 0)
    tp_place = lax.axis_index("tp")
    slot_own_base = (local_ids * sp_size + owner) * capacity + ranks
    own_slots = lax.dynamic_index_in_dim(slot_own_base, tp_place, 0, keepdims=False)
    own_rows = lax.dynamic_index_in_dim(copy_rows, tp_place, 0, keepdims=False)
    slot_count = experts_local * sp_size * capacity
    source = jnp.full((slot_count,), row_count, jnp.int32).at[own_slots].set(own_rows)
    outgoing = extended[source].reshape(experts_local, sp_size, capacity, width)
    received = lax.all_to_all(outgoing, "sp", split_axis=1, concat_axis=1, tiled=True)
    arrived = lax.all_gather(received, "tp", axis=2, tiled=True)
    expert_rows = arrived.reshape(experts_local, sp_size * tp_size * capacity, width)
    gate_part = jnp.einsum(
        "esd,edf->esf", expert_rows, gate_weight, preferred_element_type=jnp.float32
    )
    up_part = jnp.einsum("esd,edf->esf", expert_rows, up_weight, preferred_element_type=jnp.float32)
    hidden = (jax.nn.silu(gate_part) * up_part).astype(jnp.bfloat16)
    column_width = down_weight.shape[2]
    weight_rows = down_weight
    produced = jnp.einsum(
        "esf,efc->esc",
        lax.all_gather(hidden, "tp", axis=2, tiled=True),
        weight_rows,
        preferred_element_type=jnp.float32,
    ).astype(jnp.bfloat16)
    returned = lax.all_to_all(
        produced.reshape(experts_local, sp_size, tp_size * capacity, column_width),
        "sp",
        split_axis=1,
        concat_axis=1,
        tiled=True,
    )
    result_rows = returned.reshape(-1, column_width)
    picked = result_rows[slot_all.reshape(row_count, picks_count)]
    combined = jnp.sum(route_weight[:, :, None] * picked.astype(jnp.float32), 1)
    column_start = lax.axis_index("tp") * column_width
    normed_part = lax.dynamic_slice_in_dim(normed, column_start, column_width, 1)
    pre_two = ALPHA * normed_part.astype(jnp.float32) + combined
    sums, squares = packed_total((jnp.sum(pre_two, -1), jnp.sum(pre_two * pre_two, -1)), "tp")
    mean_value = (sums / width)[:, None]
    variance = (squares / width)[:, None] - mean_value * mean_value
    return ((pre_two - mean_value) * lax.rsqrt(variance + EPS) * norm_gain_two).astype(jnp.bfloat16)


def solution(mesh):
    in_specs = (
        P("sp", None),
        P("sp", "tp"),
        P("sp", "tp"),
        P("sp", "tp"),
        P("sp"),
        P("tp"),
        P(),
        P(),
        P("sp"),
        P("sp", None),
        P("sp", None),
        P("sp", None, "tp"),
        P("sp", None, "tp"),
        P("sp", None, "tp"),
        P("tp"),
    )
    out_specs = P("sp", "tp")
    return jax.shard_map(shards, mesh=mesh, in_specs=in_specs, out_specs=out_specs, check_vma=False)
```

profile of v0, /device:TPU:1, one launch (start us, length us, event | category | flops | bytes accessed | tf_op | source)
XLA Modules:
  0.0 366.8 jit_solution(6680165087132534622)
XLA Ops:
  6.5 0.8 fusion.64
  7.4 3.9 %collective-permute-start.1 = (s32[128]{0:T(128)S(1)}, s32[128]{0:T(128)S(1)}, u32[]{:S(2)}, u32[]{:S(2)}) collective-permute-start(s32[128]{0:T(128)S(1)} %get-tuple-element.16), channel_id=1, source_target_pairs={{0,8},{8,16},{16,24},{24,32},{32,40},{40,48},{48,56},{56,64},{64,7... | collective-permute-start | bytes 1544 | tf_op jit(solution)/shard_map/ppermute | solution.py:19
  11.3 1.3 collective-permute-start.3
  12.6 0.9 constant_dynamic-update-slice_fusion.1
  13.5 0.9 constant_dynamic-update-slice_fusion
  14.4 4.0 %collective-permute-start = (bf16[128,128]{0,1:T(8,128)(2,1)S(1)}, bf16[128,128]{0,1:T(8,128)(2,1)S(1)}, u32[]{:S(2)}, u32[]{:S(2)}) collective-permute-start(bf16[128,128]{0,1:T(8,128)(2,1)S(1)} %get-tuple-element.7), channel_id=1, source_target_pairs={{0,8},{8,16},{16,24},{24,32},{32,40},{40,48},{48,56},{56,64},{64,7... | collective-permute-start | bytes 98312 | tf_op jit(solution)/shard_map/ppermute | solution.py:19
  18.4 1.3 collective-permute-start.2
  19.7 0.8 fusion.65
  20.5 0.7 broadcast_multiply_fusion
  21.2 0.9 fusion.63
  22.1 0.9 copy.90
  23.0 0.2 broadcast_add_fusion
  23.2 0.2 reshape.414
  23.5 0.7 slice.98
  24.2 0.1 copy.83
  24.3 0.1 copy.87
  24.4 0.1 copy.85
  24.6 0.7 and_and_fusion.2
  25.4 0.3 fusion.67
  25.7 0.3 fusion.66
  26.1 0.2 fusion.7
  26.4 0.3 fusion.68
  26.8 0.2 fusion.8
  27.0 0.2 fusion.9
  27.2 0.1 exponential_add_fusion.1
  27.3 0.4 convolution_convert_fusion.1
  27.7 0.4 convolution_convert_fusion.3
  28.1 0.4 convolution_convert_fusion.2
  28.5 1.3 broadcast_in_dim.73
  29.7 6.0 %all-to-all-start = ((bf16[8,768,128]{1,2,0:T(8,128)(2,1)}), bf16[8,768,128]{1,2,0:T(8,128)(2,1)S(1)}, u32[]{:S(2)}, u32[]{:S(2)}) async-start(bf16[8,768,128]{1,2,0:T(8,128)(2,1)} %broadcast_in_dim.73), calls=%async_computation | async-start | bytes 3145728 | tf_op jit(solution)/shard_map/all_to_all | solution.py:29
  35.7 4.6 %reduce-window.6 = s32[8,32,2,128]{3,1,2,0:T(8,128)S(1)} reduce-window(s32[8,32,2,128]{3,1,2,0:T(8,128)S(1)} %copy_bitcast_fusion, s32[]{:T(128)} %constant.104.clone.1), window={size=1x1x1x128 pad=0_0x0_0x0_0x127_0}, to_apply=%region_8.9 | reduce-window | flops 8323072 | bytes 524292 | tf_op jit(solution)/shard_map/reduce-window
  40.4 0.1 slice.120
  40.5 0.2 copy.92
  40.7 0.1 bitcast_bitcast_fusion
  41.0 1.4 scatter_custom_fusion
  42.4 13.9 %all-to-all-done = bf16[8,768,128]{1,2,0:T(8,128)(2,1)S(1)} async-done(((bf16[8,768,128]{1,2,0:T(8,128)(2,1)}), bf16[8,768,128]{1,2,0:T(8,128)(2,1)S(1)}, u32[]{:S(2)}, u32[]{:S(2)}) %all-to-all-start) | async-done | bytes 1572896 | tf_op jit(solution)/shard_map/all_to_all | solution.py:29
  56.3 7.3 %fusion.69 = (f32[768]{0:T(1024)S(1)}, f32[768,2048]{1,0:T(8,128)S(1)}) fusion(bf16[768,1024]{0,1:T(8,128)(2,1)S(1)} %bitcast.123, bf16[1024,2048]{1,0:T(8,128)(2,1)} %param.21, bf16[768,2048]{1,0:T(8,128)(2,1)} %param.15), kind=kOutput, calls=%fused_computation.143 | convolution fusion | flops 3227516160 | bytes 15207424 | tf_op jit(solution)/shard_map/dot_general | solution.py:130
  63.7 0.8 multiply_reduce_fusion
  64.5 0.9 multiply_convert_fusion
  65.4 1.7 copy-done.1
  67.0 2.0 concatenate.32
  69.1 7.4 %gather_fusion = bf16[384,2048]{1,0:T(8,128)(2,1)} fusion(bf16[769,2048]{1,0:T(8,128)(2,1)} %concatenate.32, s32[1024]{0:T(1024)S(1)} %pad_clamp_fusion.1), kind=kCustom, calls=%fused_computation | custom fusion | bytes 3147264 | tf_op jit(solution)/shard_map/gather | solution.py:160
  76.4 2.4 reshape.420
  78.8 64.7 %all_to_all.21 = bf16[1,32,12,2048]{3,2,0,1:T(8,128)(2,1)S(1)} all-to-all(bf16[1,32,12,2048]{3,2,0,1:T(8,128)(2,1)S(1)} %bitcast.122), channel_id=1, replica_groups=mesh['sp'=32,'tp'=8] {'sp'}, dimensions={1} | all-to-all | bytes 3145728 | tf_op jit(solution)/shard_map/all_to_all | solution.py:161
  143.5 2.0 copy.96
  145.5 0.3 all-gather.6.cloned.1.call-start
  145.8 67.6 %all-gather.4.cloned.1.call-done = bf16[1,32,96,2048]{3,1,0,2:T(8,128)(2,1)} async-done(((bf16[1,32,12,2048]{3,1,0,2:T(8,128)(2,1)}), bf16[1,32,96,2048]{3,1,0,2:T(8,128)(2,1)}) %all-gather.4.cloned.1.call-update) | async-done | bytes 12582928 | tf_op jit(solution)/shard_map/all_gather | solution.py:162
  213.4 11.7 %copy.97 = bf16[1,32,96,2048]{3,2,1,0:T(8,128)(2,1)S(1)} copy(bf16[1,32,96,2048]{3,1,0,2:T(8,128)(2,1)} %all-gather.4.cloned.1.call-done) | data formatting | bytes 25165824 | tf_op jit(solution)/shard_map/all_gather | solution.py:162
  225.2 3.5 fusion.12
  228.7 4.5 %fusion = bf16[3072,128]{1,0:T(8,128)(2,1)} fusion(bf16[3072,2048]{1,0:T(8,128)(2,1)S(1)} %bitcast.121, f32[3072,128]{1,0:T(8,128)S(1)} %fusion.12, bf16[1,2048,128]{2,1,0:T(8,128)(2,1)S(1)} %copy-done.10), kind=kOutput, calls=%fused_computation.8 | convolution fusion | flops 1612972032 | bytes 15466496 | tf_op jit(solution)/shard_map/esd,edf->esf/dot_general | solution.py:167
  233.2 47.5 %all-gather.6.cloned.1.call-done = bf16[3072,1024]{1,0:T(8,128)(2,1)} async-done(((bf16[3072,128]{1,0:T(8,128)(2,1)}), bf16[3072,1024]{1,0:T(8,128)(2,1)}) %all-gather.6.cloned.1.call-update) | async-done | bytes 6291472 | tf_op jit(solution)/shard_map/all_gather | solution.py:173
  280.8 5.7 %convolution_convert_fusion = bf16[3072,256]{1,0:T(8,128)(2,1)} fusion(bf16[3072,1024]{1,0:T(8,128)(2,1)} %all-gather.6.cloned.1.call-done, bf16[1,1024,256]{2,1,0:T(8,128)(2,1)S(1)} %copy-done), kind=kOutput, calls=%fused_computation.6 | convolution fusion | flops 1611399168 | bytes 8388608 | tf_op jit(solution)/shard_map/esf,efc->esc/dot_general | solution.py:171
  286.5 9.9 %all-to-all-start.2 = ((bf16[1,32,96,256]{3,2,0,1:T(8,128)(2,1)}), bf16[1,32,96,256]{3,2,0,1:T(8,128)(2,1)S(1)}, u32[]{:S(2)}, u32[]{:S(2)}) async-start(bf16[1,32,96,256]{3,2,0,1:T(8,128)(2,1)} %bitcast.124), calls=%async_computation.2 | async-start | bytes 3145728 | tf_op jit(solution)/shard_map/all_to_all | solution.py:177
  296.4 0.3 reduce_sum.98
  296.9 0.3 compare_select_fusion
  297.1 0.2 reshape.439
  297.4 0.2 copy.89
  297.6 36.4 %all-to-all-done.2 = bf16[1,32,96,256]{3,2,0,1:T(8,128)(2,1)S(1)} async-done(((bf16[1,32,96,256]{3,2,0,1:T(8,128)(2,1)}), bf16[1,32,96,256]{3,2,0,1:T(8,128)(2,1)S(1)}, u32[]{:S(2)}, u32[]{:S(2)}) %all-to-all-start.2) | async-done | bytes 1572896 | tf_op jit(solution)/shard_map/all_to_all | solution.py:177
  334.0 5.3 %gather_fusion.1 = bf16[1536,256]{1,0:T(8,128)(2,1)} fusion(bf16[3072,256]{1,0:T(8,128)(2,1)S(1)} %bitcast.119, s32[2048]{0:T(1024)S(1)} %pad_clamp_fusion), kind=kCustom, calls=%fused_computation.1 | custom fusion | bytes 1579008 | tf_op jit(solution)/shard_map/gather | solution.py:185
  339.3 2.2 reshape.458
  341.5 4.2 %multiply_reduce_fusion.1 = f32[768,256]{1,0:T(8,128)S(1)} fusion(f32[768,2,256]{2,1,0:T(2,128)S(1)} %reshape.458, f32[768,2]{1,0:T(8,128)S(1)} %copy.89), kind=kLoop, calls=%fused_computation.9 | loop fusion | flops 589824 | bytes 2365440 | tf_op jit(solution)/shard_map/reduce_sum | solution.py:186
  345.7 1.3 fusion.19
  347.1 10.8 %all_to_all.22 = f32[8,1,1536]{2,1,0:T(1,128)S(1)} all-to-all(f32[8,1,1536]{2,1,0:T(1,128)S(1)} %broadcast_in_dim.77), channel_id=1, replica_groups=mesh['sp'=32,'tp'=8] {'tp'}, dimensions={0} | all-to-all | bytes 98304 | tf_op jit(solution)/shard_map/all_to_all | solution.py:29
  357.9 2.0 multiply_convert_fusion.1
  (59 shorter events, 0.7 us)
Async XLA Ops:
  6.5 274.2 %copy-start = (bf16[1,1024,256]{2,1,0:T(8,128)(2,1)S(1)}, bf16[1,1024,256]{2,1,0:T(8,128)(2,1)}, u32[]{:S(2)}) copy-start(bf16[1,1024,256]{2,1,0:T(8,128)(2,1)} %param.28) | copy-start | bytes 1572868
  6.5 18.0 %copy-start.4 = (s32[768]{0:T(1024)S(1)}, s32[768]{0:T(1024)}, u32[]{:S(2)}) copy-start(s32[768]{0:T(1024)} %param.19) | copy-start | bytes 9220
  6.5 18.8 %copy-start.2 = (bf16[768,64]{0,1:T(8,128)(2,1)S(1)}, bf16[768,64]{0,1:T(8,128)(2,1)}, u32[]{:S(2)}) copy-start(bf16[768,64]{0,1:T(8,128)(2,1)} %param.17) | copy-start | bytes 294916
  7.4 17.2 %collective-permute-start.1 = (s32[128]{0:T(128)S(1)}, s32[128]{0:T(128)S(1)}, u32[]{:S(2)}, u32[]{:S(2)}) collective-permute-start(s32[128]{0:T(128)S(1)} %get-tuple-element.16), channel_id=1, source_target_pairs={{0,8},{8,16},{16,24},{24,32},{32,40},{40,48},{48,56},{56,64},{64,7... | collective-permute-start | bytes 1544 | tf_op jit(solution)/shard_map/ppermute | solution.py:19
  11.3 13.3 %collective-permute-start.3 = (s32[128]{0:T(128)S(1)}, s32[128]{0:T(128)S(1)}, u32[]{:S(2)}, u32[]{:S(2)}) collective-permute-start(s32[128]{0:T(128)S(1)} %get-tuple-element.17), channel_id=1, source_target_pairs={{8,0},{16,8},{24,16},{32,24},{40,32},{48,40},{56,48},{64,56},{72,6... | collective-permute-start | bytes 1544 | tf_op jit(solution)/shard_map/ppermute | solution.py:22
  14.4 11.7 %copy-start.7 = (f32[2]{0:T(128)S(1)}, f32[2]{0:T(128)}, u32[]{:S(2)}) copy-start(f32[2]{0:T(128)} %param.20) | copy-start | bytes 28
  14.4 11.3 %collective-permute-start = (bf16[128,128]{0,1:T(8,128)(2,1)S(1)}, bf16[128,128]{0,1:T(8,128)(2,1)S(1)}, u32[]{:S(2)}, u32[]{:S(2)}) collective-permute-start(bf16[128,128]{0,1:T(8,128)(2,1)S(1)} %get-tuple-element.7), channel_id=1, source_target_pairs={{0,8},{8,16},{16,24},{24,32},{32,40},{40,48},{48,56},{56,64},{64,7... | collective-permute-start | bytes 98312 | tf_op jit(solution)/shard_map/ppermute | solution.py:19
  18.4 7.9 %collective-permute-start.2 = (bf16[128,128]{0,1:T(8,128)(2,1)S(1)}, bf16[128,128]{0,1:T(8,128)(2,1)S(1)}, u32[]{:S(2)}, u32[]{:S(2)}) collective-permute-start(bf16[128,128]{0,1:T(8,128)(2,1)S(1)} %get-tuple-element.8), channel_id=1, source_target_pairs={{8,0},{16,8},{24,16},{32,24},{40,32},{48,40},{56,48},{64,56},{72,6... | collective-permute-start | bytes 98312 | tf_op jit(solution)/shard_map/ppermute | solution.py:22
  25.7 1.6 copy-start.3
  29.7 26.6 %all-to-all-start = ((bf16[8,768,128]{1,2,0:T(8,128)(2,1)}), bf16[8,768,128]{1,2,0:T(8,128)(2,1)S(1)}, u32[]{:S(2)}, u32[]{:S(2)}) async-start(bf16[8,768,128]{1,2,0:T(8,128)(2,1)} %broadcast_in_dim.73), calls=%async_computation | async-start | bytes 3145728 | tf_op jit(solution)/shard_map/all_to_all | solution.py:29
  35.7 177.7 %all-gather.4.cloned.1.call-start = ((), (), s32[]{:S(2)}) async-start(), calls=%async_computation.4 | async-start | bytes 14155776 | tf_op jit(solution)/shard_map/all_gather | solution.py:162
  63.7 0.8 copy-start.5
  65.3 1.7 copy-start.1
  145.5 79.6 %copy-start.9 = (bf16[1,2048,128]{2,1,0:T(8,128)(2,1)S(1)}, bf16[1,2048,128]{2,1,0:T(8,128)(2,1)}, u32[]{:S(2)}) copy-start(bf16[1,2048,128]{2,1,0:T(8,128)(2,1)} %param.26) | copy-start | bytes 1572868
  145.5 135.3 %all-gather.6.cloned.1.call-start = ((), (), s32[]{:S(2)}) async-start(), calls=%async_computation.5 | async-start | bytes 7077888 | tf_op jit(solution)/shard_map/all_gather | solution.py:173
  225.1 3.6 copy-start.10
  286.5 10.9 %copy-start.6 = (f32[768,2]{0,1:T(2,128)S(1)}, f32[768,2]{0,1:T(2,128)}, u32[]{:S(2)}) copy-start(f32[768,2]{0,1:T(2,128)} %param.25) | copy-start | bytes 18436
  286.5 47.5 %all-to-all-start.2 = ((bf16[1,32,96,256]{3,2,0,1:T(8,128)(2,1)}), bf16[1,32,96,256]{3,2,0,1:T(8,128)(2,1)S(1)}, u32[]{:S(2)}, u32[]{:S(2)}) async-start(bf16[1,32,96,256]{3,2,0,1:T(8,128)(2,1)} %bitcast.124), calls=%async_computation.2 | async-start | bytes 3145728 | tf_op jit(solution)/shard_map/all_to_all | solution.py:177
  339.3 18.6 %copy-start.8 = (f32[256]{0:T(256)S(1)}, f32[256]{0:T(256)}, u32[]{:S(2)}) copy-start(f32[256]{0:T(256)} %param.29) | copy-start | bytes 3076
Sparse Core Ops, SparseCore 0:
  145.6 67.7 all-gather.3
  233.3 47.3 all-gather.5
where the time goes:
time: 368 us; the launch traced here: 367 us
  waiting for transfers between devices  166 us (45%)
  blocking collectives  75.4 us (20%)
  local copies, waits for them, and re-layouts  44.9 us (12%)
  starting transfers between devices  26.7 us (7%)
  matrix products  23.2 us (6%)
  other arithmetic  17 us (5%)
  between operations  14 us (4%)
    all_gather x1, waiting for transfers between devices, shards(): arrived = lax.all_gather(received, 'tp', axis=2, tiled=True)  67.6 us
    all_to_all x1, blocking collectives, shards(): lax.all_to_all(outgoing, 'sp', split_axis=1, concat_axis=1, tiled=True)  64.7 us
    all_gather x1, waiting for transfers between devices, shards(): lax.all_gather(hidden, 'tp', axis=2, tiled=True)  47.5 us
    all_to_all x1, waiting for transfers between devices, shards(): lax.all_to_all(produced.reshape(experts_local, sp_size, tp_size * capacit...  36.4 us
    all_to_all x1, waiting for transfers between devices, copy_for_each(): return lax.all_to_all(copies, axis, split_axis=0, concat_axis=0, tiled=True)  13.9 us
    all_gather x1, local copies, waits for them, and re-layouts, shards(): arrived = lax.all_gather(received, 'tp', axis=2, tiled=True)  11.7 us
    all_to_all x1, blocking collectives, copy_for_each(): return lax.all_to_all(copies, axis, split_axis=0, concat_axis=0, tiled=True)  10.8 us
    all_to_all x1, starting transfers between devices, shards(): lax.all_to_all(produced.reshape(experts_local, sp_size, tp_size * capacit...  9.93 us
  transfers between devices with their start and end apart: 8, of which 4 were waited for; matrix products, arithmetic and copies ran while one was open for 4% of the time, Pallas kernels for 0%

commit v1 on v0

--- a/solution.py
+++ b/solution.py
@@ -174,12 +174,20 @@
         weight_rows,
         preferred_element_type=jnp.float32,
     ).astype(jnp.bfloat16)
-    returned = lax.all_to_all(
-        produced.reshape(experts_local, sp_size, tp_size * capacity, column_width),
-        "sp",
-        split_axis=1,
-        concat_axis=1,
-        tiled=True,
+    returned = jnp.concatenate(
+        lax.all_to_all(
+            jnp.stack(
+                jnp.split(
+                    produced.reshape(experts_local, sp_size, tp_size * capacity, column_width),
+                    lax.axis_size("sp"),
+                    axis=1,
+                )
+            ),
+            "sp",
+            0,
+            0,
+        ),
+        axis=1,
     )
     result_rows = returned.reshape(-1, column_width)
     picked = result_rows[slot_all.reshape(row_count, picks_count)]

time: 368 us -> 386 us (1.049)
  local copies, waits for them, and re-layouts: 44.9 us -> 64.3 us
    unnamed x25 -> x56, local copies, waits for them, and re-layouts: 3.66 us -> 23.1 us
where the time goes in v1:
time: 386 us; the launch traced here: 385 us
  waiting for transfers between devices  166 us (43%)
  blocking collectives  75.4 us (20%)
  local copies, waits for them, and re-layouts  64.3 us (17%)
  starting transfers between devices  26.5 us (7%)
  matrix products  22.1 us (6%)
  other arithmetic  17 us (4%)
  between operations  14 us (4%)
    all_gather x1, waiting for transfers between devices, shards(): arrived = lax.all_gather(received, 'tp', axis=2, tiled=True)  67.6 us
    all_to_all x1, blocking collectives, shards(): lax.all_to_all(outgoing, 'sp', split_axis=1, concat_axis=1, tiled=True)  64.7 us
    all_gather x1, waiting for transfers between devices, shards(): lax.all_gather(hidden, 'tp', axis=2, tiled=True)  47.5 us
    all_to_all x1, waiting for transfers between devices, shards(): lax.all_to_all(jnp.stack(jnp.split(produced.reshape(experts_local, sp_siz...  36.4 us
    unnamed x56, local copies, waits for them, and re-layouts  23.1 us
    all_to_all x1, waiting for transfers between devices, copy_for_each(): return lax.all_to_all(copies, axis, split_axis=0, concat_axis=0, tiled=True)  13.9 us
    all_gather x1, local copies, waits for them, and re-layouts, shards(): arrived = lax.all_gather(received, 'tp', axis=2, tiled=True)  11.7 us
    all_to_all x1, blocking collectives, copy_for_each(): return lax.all_to_all(copies, axis, split_axis=0, concat_axis=0, tiled=True)  10.8 us
  transfers between devices with their start and end apart: 8, of which 4 were waited for; matrix products, arithmetic and copies ran while one was open for 4% of the time, Pallas kernels for 0%

profile of v1, /device:TPU:1, one launch (start us, length us, event | category | flops | bytes accessed | tf_op | source)
XLA Modules:
  0.0 384.9 jit_solution(12500748093466137066)
XLA Ops:
  6.5 0.8 fusion.64
  7.3 3.9 %collective-permute-start.1 = (s32[128]{0:T(128)S(1)}, s32[128]{0:T(128)S(1)}, u32[]{:S(2)}, u32[]{:S(2)}) collective-permute-start(s32[128]{0:T(128)S(1)} %get-tuple-element.16), channel_id=1, source_target_pairs={{0,8},{8,16},{16,24},{24,32},{32,40},{40,48},{48,56},{56,64},{64,7... | collective-permute-start | bytes 1544 | tf_op jit(solution)/shard_map/ppermute | solution.py:19
  11.3 1.3 collective-permute-start.3
  12.6 0.9 constant_dynamic-update-slice_fusion.1
  13.5 0.9 constant_dynamic-update-slice_fusion
  14.4 4.0 %collective-permute-start = (bf16[128,128]{0,1:T(8,128)(2,1)S(1)}, bf16[128,128]{0,1:T(8,128)(2,1)S(1)}, u32[]{:S(2)}, u32[]{:S(2)}) collective-permute-start(bf16[128,128]{0,1:T(8,128)(2,1)S(1)} %get-tuple-element.7), channel_id=1, source_target_pairs={{0,8},{8,16},{16,24},{24,32},{32,40},{40,48},{48,56},{56,64},{64,7... | collective-permute-start | bytes 98312 | tf_op jit(solution)/shard_map/ppermute | solution.py:19
  18.4 1.3 collective-permute-start.2
  19.7 0.8 fusion.65
  20.5 0.7 broadcast_multiply_fusion
  21.2 0.9 fusion.63
  22.1 0.9 copy.87
  24.0 0.7 and_and_fusion.2
  28.1 1.3 broadcast_in_dim.73
  29.3 6.0 %all-to-all-start = ((bf16[8,768,128]{1,2,0:T(8,128)(2,1)}), bf16[8,768,128]{1,2,0:T(8,128)(2,1)S(1)}, u32[]{:S(2)}, u32[]{:S(2)}) async-start(bf16[8,768,128]{1,2,0:T(8,128)(2,1)} %broadcast_in_dim.73), calls=%async_computation | async-start | bytes 3145728 | tf_op jit(solution)/shard_map/all_to_all | solution.py:29
  35.3 4.6 %reduce-window.6 = s32[8,32,2,128]{3,1,2,0:T(8,128)S(1)} reduce-window(s32[8,32,2,128]{3,1,2,0:T(8,128)S(1)} %copy_bitcast_fusion, s32[]{:T(128)} %constant.104.clone.1), window={size=1x1x1x128 pad=0_0x0_0x0_0x127_0}, to_apply=%region_8.9 | reduce-window | flops 8323072 | bytes 524292 | tf_op jit(solution)/shard_map/reduce-window
  40.6 1.4 scatter_custom_fusion
  42.0 13.9 %all-to-all-done = bf16[8,768,128]{1,2,0:T(8,128)(2,1)S(1)} async-done(((bf16[8,768,128]{1,2,0:T(8,128)(2,1)}), bf16[8,768,128]{1,2,0:T(8,128)(2,1)S(1)}, u32[]{:S(2)}, u32[]{:S(2)}) %all-to-all-start) | async-done | bytes 1572896 | tf_op jit(solution)/shard_map/all_to_all | solution.py:29
  55.9 7.3 %fusion.69 = (f32[768]{0:T(1024)S(1)}, f32[768,2048]{1,0:T(8,128)S(1)}) fusion(bf16[768,1024]{0,1:T(8,128)(2,1)S(1)} %bitcast.249, bf16[1024,2048]{1,0:T(8,128)(2,1)} %param.21, bf16[768,2048]{1,0:T(8,128)(2,1)} %param.15), kind=kOutput, calls=%fused_computation.207 | convolution fusion | flops 3227516160 | bytes 15207424 | tf_op jit(solution)/shard_map/dot_general | solution.py:130
  63.3 0.8 multiply_reduce_fusion
  64.0 0.9 multiply_convert_fusion
  64.9 1.7 copy-done.1
  66.6 2.0 concatenate.32
  68.6 7.4 %gather_fusion = bf16[384,2048]{1,0:T(8,128)(2,1)} fusion(bf16[769,2048]{1,0:T(8,128)(2,1)} %concatenate.32, s32[1024]{0:T(1024)S(1)} %pad_clamp_fusion.1), kind=kCustom, calls=%fused_computation | custom fusion | bytes 3147264 | tf_op jit(solution)/shard_map/gather | solution.py:160
  76.0 2.4 reshape.417
  78.4 64.7 %all_to_all.21 = bf16[1,32,12,2048]{3,2,0,1:T(8,128)(2,1)S(1)} all-to-all(bf16[1,32,12,2048]{3,2,0,1:T(8,128)(2,1)S(1)} %bitcast.248), channel_id=1, replica_groups=mesh['sp'=32,'tp'=8] {'sp'}, dimensions={1} | all-to-all | bytes 3145728 | tf_op jit(solution)/shard_map/all_to_all | solution.py:161
  143.0 2.0 copy.93
  145.4 67.6 %all-gather.4.cloned.1.call-done = bf16[1,32,96,2048]{3,1,0,2:T(8,128)(2,1)} async-done(((bf16[1,32,12,2048]{3,1,0,2:T(8,128)(2,1)}), bf16[1,32,96,2048]{3,1,0,2:T(8,128)(2,1)}) %all-gather.4.cloned.1.call-update) | async-done | bytes 12582928 | tf_op jit(solution)/shard_map/all_gather | solution.py:162
  213.0 11.7 %copy.94 = bf16[1,32,96,2048]{3,2,1,0:T(8,128)(2,1)S(1)} copy(bf16[1,32,96,2048]{3,1,0,2:T(8,128)(2,1)} %all-gather.4.cloned.1.call-done) | data formatting | bytes 25165824 | tf_op jit(solution)/shard_map/all_gather | solution.py:162
  224.7 3.5 fusion.12
  228.3 4.5 %fusion = bf16[3072,128]{1,0:T(8,128)(2,1)} fusion(bf16[3072,2048]{1,0:T(8,128)(2,1)S(1)} %bitcast.247, f32[3072,128]{1,0:T(8,128)S(1)} %fusion.12, bf16[1,2048,128]{2,1,0:T(8,128)(2,1)S(1)} %copy-done.10), kind=kOutput, calls=%fused_computation.8 | convolution fusion | flops 1612972032 | bytes 15466496 | tf_op jit(solution)/shard_map/esd,edf->esf/dot_general | solution.py:167
  232.8 47.5 %all-gather.6.cloned.1.call-done = bf16[3072,1024]{1,0:T(8,128)(2,1)} async-done(((bf16[3072,128]{1,0:T(8,128)(2,1)}), bf16[3072,1024]{1,0:T(8,128)(2,1)}) %all-gather.6.cloned.1.call-update) | async-done | bytes 6291472 | tf_op jit(solution)/shard_map/all_gather | solution.py:173
  280.3 4.6 %convolution_convert_fusion = bf16[3072,256]{1,0:T(8,128)(2,1)S(1)} fusion(bf16[3072,1024]{1,0:T(8,128)(2,1)} %all-gather.6.cloned.1.call-done, bf16[1,1024,256]{2,1,0:T(8,128)(2,1)S(1)} %copy-done), kind=kOutput, calls=%fused_computation.6 | convolution fusion | flops 1611399168 | bytes 8388608 | tf_op jit(solution)/shard_map/esf,efc->esc/dot_general | solution.py:171
  284.9 0.6 constant_dynamic-update-slice_fusion.33
  286.2 0.6 constant_dynamic-update-slice_fusion.31
  286.8 0.6 constant_dynamic-update-slice_fusion.30
  287.4 0.6 constant_dynamic-update-slice_fusion.29
  288.6 0.6 constant_dynamic-update-slice_fusion.27
  289.9 0.6 constant_dynamic-update-slice_fusion.25
  290.5 0.6 constant_dynamic-update-slice_fusion.24
  291.7 0.6 constant_dynamic-update-slice_fusion.22
  292.4 0.6 constant_dynamic-update-slice_fusion.21
  293.0 0.6 constant_dynamic-update-slice_fusion.20
  293.6 0.6 constant_dynamic-update-slice_fusion.19
  294.2 0.6 constant_dynamic-update-slice_fusion.18
  294.8 0.6 constant_dynamic-update-slice_fusion.17
  295.4 0.6 constant_dynamic-update-slice_fusion.16
  296.1 0.6 constant_dynamic-update-slice_fusion.15
  296.7 0.6 constant_dynamic-update-slice_fusion.14
  297.3 0.6 constant_dynamic-update-slice_fusion.13
  298.5 0.6 constant_dynamic-update-slice_fusion.11
  299.8 0.6 constant_dynamic-update-slice_fusion.9
  300.4 0.6 constant_dynamic-update-slice_fusion.8
  301.0 0.6 constant_dynamic-update-slice_fusion.7
  302.3 0.6 constant_dynamic-update-slice_fusion.5
  303.5 0.6 constant_dynamic-update-slice_fusion.3
  304.1 0.6 constant_dynamic-update-slice_fusion.2
  304.7 9.8 %all-to-all-start.2 = ((bf16[32,1,1,96,256]{4,3,2,1,0:T(8,128)(2,1)}), bf16[32,1,1,96,256]{4,3,2,1,0:T(8,128)(2,1)S(1)}, u32[]{:S(2)}, u32[]{:S(2)}) async-start(bf16[32,1,1,96,256]{4,3,2,1,0:T(8,128)(2,1)} %constant_dynamic-update-slice_fusion.2), calls=%async_computation.2 | async-start | bytes 3145728 | tf_op jit(solution)/shard_map/all_to_all | solution.py:178
  315.7 36.4 %all-to-all-done.2 = bf16[32,1,1,96,256]{4,3,2,1,0:T(8,128)(2,1)S(1)} async-done(((bf16[32,1,1,96,256]{4,3,2,1,0:T(8,128)(2,1)}), bf16[32,1,1,96,256]{4,3,2,1,0:T(8,128)(2,1)S(1)}, u32[]{:S(2)}, u32[]{:S(2)}) %all-to-all-start.2) | async-done | bytes 1572896 | tf_op jit(solution)/shard_map/all_to_all | solution.py:178
  352.1 5.3 %gather_fusion.1 = bf16[1536,256]{1,0:T(8,128)(2,1)} fusion(bf16[3072,256]{1,0:T(8,128)(2,1)S(1)} %bitcast.245, s32[2048]{0:T(1024)S(1)} %pad_clamp_fusion), kind=kCustom, calls=%fused_computation.1 | custom fusion | bytes 1579008 | tf_op jit(solution)/shard_map/gather | solution.py:193
  357.4 2.1 reshape.454
  359.6 4.2 %multiply_reduce_fusion.1 = f32[768,256]{1,0:T(8,128)S(1)} fusion(f32[768,2,256]{2,1,0:T(2,128)S(1)} %reshape.454, f32[768,2]{1,0:T(8,128)S(1)} %copy.86), kind=kLoop, calls=%fused_computation.9 | loop fusion | flops 589824 | bytes 2365440 | tf_op jit(solution)/shard_map/reduce_sum | solution.py:194
  363.8 1.3 fusion.19
  365.2 10.8 %all_to_all.22 = f32[8,1,1536]{2,1,0:T(1,128)S(1)} all-to-all(f32[8,1,1536]{2,1,0:T(1,128)S(1)} %broadcast_in_dim.77), channel_id=1, replica_groups=mesh['sp'=32,'tp'=8] {'tp'}, dimensions={0} | all-to-all | bytes 98304 | tf_op jit(solution)/shard_map/all_to_all | solution.py:29
  376.0 2.0 multiply_convert_fusion.1
  (91 shorter events, 11.2 us)
Async XLA Ops:
  6.5 273.8 %copy-start = (bf16[1,1024,256]{2,1,0:T(8,128)(2,1)S(1)}, bf16[1,1024,256]{2,1,0:T(8,128)(2,1)}, u32[]{:S(2)}) copy-start(bf16[1,1024,256]{2,1,0:T(8,128)(2,1)} %param.28) | copy-start | bytes 1572868
  6.5 17.0 %copy-start.4 = (s32[768]{0:T(1024)S(1)}, s32[768]{0:T(1024)}, u32[]{:S(2)}) copy-start(s32[768]{0:T(1024)} %param.19) | copy-start | bytes 9220
  7.3 16.5 %collective-permute-start.1 = (s32[128]{0:T(128)S(1)}, s32[128]{0:T(128)S(1)}, u32[]{:S(2)}, u32[]{:S(2)}) collective-permute-start(s32[128]{0:T(128)S(1)} %get-tuple-element.16), channel_id=1, source_target_pairs={{0,8},{8,16},{16,24},{24,32},{32,40},{40,48},{48,56},{56,64},{64,7... | collective-permute-start | bytes 1544 | tf_op jit(solution)/shard_map/ppermute | solution.py:19
  11.3 12.6 %collective-permute-start.3 = (s32[128]{0:T(128)S(1)}, s32[128]{0:T(128)S(1)}, u32[]{:S(2)}, u32[]{:S(2)}) collective-permute-start(s32[128]{0:T(128)S(1)} %get-tuple-element.17), channel_id=1, source_target_pairs={{8,0},{16,8},{24,16},{32,24},{40,32},{48,40},{56,48},{64,56},{72,6... | collective-permute-start | bytes 1544 | tf_op jit(solution)/shard_map/ppermute | solution.py:22
  14.4 10.6 %collective-permute-start = (bf16[128,128]{0,1:T(8,128)(2,1)S(1)}, bf16[128,128]{0,1:T(8,128)(2,1)S(1)}, u32[]{:S(2)}, u32[]{:S(2)}) collective-permute-start(bf16[128,128]{0,1:T(8,128)(2,1)S(1)} %get-tuple-element.7), channel_id=1, source_target_pairs={{0,8},{8,16},{16,24},{24,32},{32,40},{40,48},{48,56},{56,64},{64,7... | collective-permute-start | bytes 98312 | tf_op jit(solution)/shard_map/ppermute | solution.py:19
  18.4 7.3 %collective-permute-start.2 = (bf16[128,128]{0,1:T(8,128)(2,1)S(1)}, bf16[128,128]{0,1:T(8,128)(2,1)S(1)}, u32[]{:S(2)}, u32[]{:S(2)}) collective-permute-start(bf16[128,128]{0,1:T(8,128)(2,1)S(1)} %get-tuple-element.8), channel_id=1, source_target_pairs={{8,0},{16,8},{24,16},{32,24},{40,32},{48,40},{56,48},{64,56},{72,6... | collective-permute-start | bytes 98312 | tf_op jit(solution)/shard_map/ppermute | solution.py:22
  21.2 3.5 copy-start.2
  23.9 1.4 copy-start.7
  26.0 0.9 copy-start.3
  29.3 26.6 %all-to-all-start = ((bf16[8,768,128]{1,2,0:T(8,128)(2,1)}), bf16[8,768,128]{1,2,0:T(8,128)(2,1)S(1)}, u32[]{:S(2)}, u32[]{:S(2)}) async-start(bf16[8,768,128]{1,2,0:T(8,128)(2,1)} %broadcast_in_dim.73), calls=%async_computation | async-start | bytes 3145728 | tf_op jit(solution)/shard_map/all_to_all | solution.py:29
  35.3 177.7 %all-gather.4.cloned.1.call-start = ((), (), s32[]{:S(2)}) async-start(), calls=%async_computation.4 | async-start | bytes 14155776 | tf_op jit(solution)/shard_map/all_gather | solution.py:162
  63.2 0.8 copy-start.5
  64.9 1.7 copy-start.1
  145.1 79.6 %copy-start.9 = (bf16[1,2048,128]{2,1,0:T(8,128)(2,1)S(1)}, bf16[1,2048,128]{2,1,0:T(8,128)(2,1)}, u32[]{:S(2)}) copy-start(bf16[1,2048,128]{2,1,0:T(8,128)(2,1)} %param.26) | copy-start | bytes 1572868
  145.1 135.2 %all-gather.6.cloned.1.call-start = ((), (), s32[]{:S(2)}) async-start(), calls=%async_computation.5 | async-start | bytes 7077888 | tf_op jit(solution)/shard_map/all_gather | solution.py:173
  224.7 3.6 copy-start.10
  304.7 47.4 %all-to-all-start.2 = ((bf16[32,1,1,96,256]{4,3,2,1,0:T(8,128)(2,1)}), bf16[32,1,1,96,256]{4,3,2,1,0:T(8,128)(2,1)S(1)}, u32[]{:S(2)}, u32[]{:S(2)}) async-start(bf16[32,1,1,96,256]{4,3,2,1,0:T(8,128)(2,1)} %constant_dynamic-update-slice_fusion.2), calls=%async_computation.2 | async-start | bytes 3145728 | tf_op jit(solution)/shard_map/all_to_all | solution.py:178
  314.5 0.9 copy-start.6
  359.6 16.4 %copy-start.8 = (f32[256]{0:T(256)S(1)}, f32[256]{0:T(256)}, u32[]{:S(2)}) copy-start(f32[256]{0:T(256)} %param.29) | copy-start | bytes 3076
Sparse Core Ops, SparseCore 0:
  145.2 67.7 all-gather.3
  232.9 47.3 all-gather.5
